TPU v7x, 128 devices: a whole 4x4x4 slice. The times are simulated.
128 devices in a mesh: sp: 16 (over z, x), fs: 4 (over y), tp: 2 (over core).
Axes of the slice: x: 4, y: 4, z: 4, core: 2. Of those that a mesh axis runs over, the one named last changes fastest.
Arguments:
- stream: bfloat16 [4, 16384, 2048], P('fs', 'sp', 'tp'), parts along dimension 0, may hold values from -6 to 6
- w_pool_in: bfloat16 [2048, 1024], P(None, 'tp'), may hold values from -0.125 to 0.125
- w_query: bfloat16 [2048, 1024], P(None, 'tp'), may hold values from -0.125 to 0.125
- w_forget: bfloat16 [2048, 1024], P(None, 'tp'), may hold values from -0.125 to 0.125
- w_value: bfloat16 [2048, 1024], P(None, 'tp'), may hold values from -0.125 to 0.125
- w_outgate: bfloat16 [2048, 1024], P(None, 'tp'), may hold values from -0.125 to 0.125
- pool_mix: bfloat16 [4, 256, 256], P('tp'), may hold values from -0.375 to 0.375
- pool_scale: float32 [1024], P('tp'), may hold values from 0.1 to 1.9
- lower_bound: float32 [1024], P('tp'), may hold values from 0.9 to 1
- extra_decay: float32 [16384, 8], P('sp', 'tp'), may hold values from -0.7 to 0
- rec_gain: float32 [128], replicated, may hold values from 0.1 to 1.9
- w_out_pool: bfloat16 [1024, 2048], P('tp'), may hold values from -0.125 to 0.125
- w_out_rec: bfloat16 [1024, 2048], P('tp'), may hold values from -0.125 to 0.125
- norm_gain: float32 [2048], P('tp'), may hold values from 0.1 to 1.9
- norm_bias: float32 [2048], P('tp'), may hold values from -3 to 3
Outputs:
- layer_out: bfloat16 [4, 16384, 2048], P('fs', 'sp', 'tp'), parts along dimension 0
There are 4 independent parts, one for each index of `fs`. A program takes and returns all parts, laid end to end along the dimension named above; an argument that names none is the same for every part. Nothing has to cross between parts.
All inputs are finite; a program needn't handle non-finite values.
Results may differ from a plain program's by a relative error of at most 0.0085.
Values may be sent and summed in bfloat16 or wider, within the bound.
No kernel may reach another device: no remote copies, remote signals or barrier semaphores. Data moves between devices by JAX's collectives and lax.ppermute only.
A program may use at most 128 MiB of HBM per device.

v0:
```python
import jax
import jax.numpy as jnp
from jax import lax
from jax.sharding import Mesh
from jax.sharding import PartitionSpec as P

D = 2048
DK = 128
WMAX = 16
BLOCK_ROWS = 128
GROUP_CH = 256
SP = ("sp_0", "sp_1")
ALPHA = 2.0**0.25
EPS_RMS = 1e-06
EPS_NORM = 1e-05


def filled_with(x, identity):
    return jax.tree.map(
        lambda a, e: jnp.broadcast_to(jnp.asarray(e, a.dtype), a.shape), x, identity
    )


def gathered_once(x, axis):
    leaves = jax.tree.leaves(x)
    turns = sorted(range(len(leaves)), key=lambda k: -leaves[k].size)
    width = (1, *leaves[turns[0]].shape)[-1]
    lines = [
        jnp.pad(leaves[k].reshape(-1), (0, -leaves[k].size % width)).reshape(-1, width)
        for k in turns
    ]
    both, at, found = (lax.all_gather(jnp.concatenate(lines), axis), 0, {})
    for k, line in zip(turns, lines):
        section = both[:, at : at + len(line)].reshape(len(both), -1)
        found[k] = section[:, : leaves[k].size].reshape(-1, *leaves[k].shape)
        at += len(line)
    numbers = iter(range(len(leaves)))
    return jax.tree.map(lambda _: found[next(numbers)], x)


def entering(x, axes, combine, identity):
    before = start = filled_with(x, identity)
    subtotal = x
    for axis in reversed(axes):
        devices, mine = (lax.axis_size(axis), lax.axis_index(axis))
        pieces = gathered_once(
            jax.tree.map(
                lambda part, kind: part.astype(kind),
                subtotal,
                (jnp.bfloat16, jnp.bfloat16, jnp.bfloat16, jnp.bfloat16),
            ),
            axis,
        )
        inside, subtotal = (start, start)
        for k in range(devices):
            passed = k < mine
            subtotal = combine(
                subtotal, jax.tree.map(lambda part, own: part[k].astype(own.dtype), pieces, x)
            )
            inside = jax.tree.map(lambda new, old: jnp.where(passed, new, old), subtotal, inside)
        before = combine(inside, before)
    return before


def split_up(x, dim, devices):
    before, after = (x.shape[:dim], x.shape[dim + 1 :])
    return jnp.moveaxis(x.reshape(*before, devices, -1, *after), dim, 0)


def summed_on_arrival(x, axis, dim):
    devices = lax.axis_size(axis)
    pieces = lax.all_to_all(split_up(x, dim, devices), axis, 0, 0, tiled=True)
    return jnp.sum(pieces, axis=0)


def total_of_pieces(x, axis):
    pieces = lax.all_gather(x, axis)
    return pieces.sum(axis=0)


def local(
    stream,
    w_pool_in,
    w_query,
    w_forget,
    w_value,
    w_outgate,
    pool_mix,
    pool_scale,
    lower_bound,
    extra_decay,
    rec_gain,
    w_out_pool,
    w_out_rec,
    norm_gain,
    norm_bias,
):
    features = stream[0]
    length = features.shape[0]
    weights = (w_pool_in, w_query, w_forget, w_value, w_outgate)
    column_piece = lax.all_gather(features, "tp", axis=1, tiled=True)
    projected = tuple(
        (jnp.dot(column_piece, weight, preferred_element_type=jnp.float32) for weight in weights)
    )
    pooled, queries, forget_in, value_in, gate_in = [
        projection.astype(jnp.bfloat16) for projection in projected
    ]
    pool_width = pooled.shape[1]
    tail_rows = pooled[length - (WMAX - 1) :]
    channels = lower_bound.shape[0]
    heads_here = channels // DK
    blocks = length // BLOCK_ROWS
    forget = lower_bound + (1.0 - lower_bound) * jax.nn.sigmoid(forget_in.astype(jnp.float32))
    log_keep = (jnp.log(forget).reshape(length, heads_here, DK) + extra_decay[:, :, None]).reshape(
        length, channels
    )
    weight_in = 1.0 - forget
    squashed = jax.nn.silu(queries.astype(jnp.float32))
    row_ids = lax.broadcasted_iota(jnp.int32, (BLOCK_ROWS, BLOCK_ROWS), 0)
    col_ids = lax.broadcasted_iota(jnp.int32, (BLOCK_ROWS, BLOCK_ROWS), 1)
    lower_mask = (row_ids >= col_ids).astype(jnp.float32)
    keep_blocks = log_keep.reshape(blocks, BLOCK_ROWS, channels)
    log_total = jnp.einsum("ts,bsc->btc", lower_mask, keep_blocks)
    log_end = log_total[:, BLOCK_ROWS - 1]
    query_blocks = squashed.reshape(blocks, BLOCK_ROWS, channels)
    input_blocks = weight_in.reshape(blocks, BLOCK_ROWS, channels)
    value_heads = value_in.reshape(blocks, BLOCK_ROWS, heads_here, DK)
    query_up = (query_blocks * jnp.exp(log_total)).reshape(blocks, BLOCK_ROWS, heads_here, DK)
    input_down = (input_blocks * jnp.exp(-log_total)).reshape(blocks, BLOCK_ROWS, heads_here, DK)
    scores = jnp.einsum("bthd,bshd->bhts", query_up, input_down) * lower_mask[None, None]
    inside = jnp.einsum(
        "bhts,bshe->bthe",
        scores.astype(jnp.bfloat16),
        value_heads,
        preferred_element_type=jnp.float32,
    )
    in_weight = (input_blocks * jnp.exp(log_end[:, None] - log_total)).astype(jnp.bfloat16)
    own_terms = jnp.einsum(
        "bshd,bshe->bhde",
        in_weight.reshape(blocks, BLOCK_ROWS, heads_here, DK),
        value_heads,
        preferred_element_type=jnp.float32,
    )

    def block_step(carry, inputs):
        state, offset = carry
        end_blk, term_blk = inputs
        new_state = jnp.exp(end_blk).reshape(heads_here, DK)[:, :, None] * state + term_blk
        return ((new_state, offset + end_blk), (state, offset))

    start_carry = (
        jnp.zeros((heads_here, DK, DK), jnp.float32),
        jnp.zeros((channels,), jnp.float32),
    )
    final_carry, befores = lax.scan(block_step, start_carry, (log_end, own_terms))
    states_before, offsets_before = befores
    carried = jnp.einsum("bthd,bhde->bthe", query_up, states_before)
    local_out = (inside + carried).reshape(length, heads_here, DK)
    query_far = (query_blocks * jnp.exp(offsets_before[:, None] + log_total)).reshape(
        length, heads_here, DK
    )
    local_state = final_carry[0]
    local_keep = jnp.exp(final_carry[1]).reshape(heads_here, DK)
    unit_keep = jnp.ones_like(local_keep)
    empty_state = jnp.zeros_like(local_state)

    def join_all(earlier, later):
        present = later[3] > 0
        return (
            earlier[0] * later[0],
            later[0][:, :, None] * earlier[1] + later[1],
            jnp.where(present, later[2], earlier[2]),
            jnp.maximum(earlier[3], later[3]),
        )

    empty_rows = jnp.zeros(tail_rows.shape, jnp.float32)
    scanned = entering(
        (local_keep, local_state, tail_rows.astype(jnp.float32), jnp.ones((1,), jnp.float32)),
        SP,
        join_all,
        (unit_keep, empty_state, empty_rows, jnp.zeros((1,), jnp.float32)),
    )
    incoming = scanned[1]
    halo_rows = scanned[2].astype(jnp.bfloat16)
    rec_raw = local_out + jnp.einsum("thd,hde->the", query_far, incoming)
    rec_norm = (
        rec_raw
        * lax.rsqrt(jnp.mean(rec_raw * rec_raw, axis=-1, keepdims=True) + EPS_RMS)
        * rec_gain
    )
    gated = rec_norm * jax.nn.silu(gate_in.astype(jnp.float32)).reshape(length, heads_here, DK)
    rec_out = gated.reshape(length, channels).astype(jnp.bfloat16)
    padded = jnp.concatenate([halo_rows, pooled], axis=0).astype(jnp.float32)
    channel_ids = lax.axis_index("tp") * pool_width + lax.iota(jnp.int32, pool_width)
    group_id = channel_ids // GROUP_CH
    window_len = jnp.left_shift(jnp.ones_like(group_id), group_id + 1)
    window_sum = jnp.zeros((length, pool_width), jnp.float32)
    for lag_rows in range(WMAX):
        lagged = padded[WMAX - 1 - lag_rows : WMAX - 1 - lag_rows + length]
        window_sum = window_sum + jnp.where(
            lag_rows < window_len[None, :], lagged, jnp.float32(0.0)
        )
    position = (lax.axis_index(SP) * length + lax.iota(jnp.int32, length) + 1).astype(jnp.float32)
    counts = jnp.minimum(position[:, None], window_len.astype(jnp.float32)[None, :])
    pool_diff = (window_sum / counts - pooled.astype(jnp.float32)).astype(jnp.bfloat16)
    groups_here = pool_mix.shape[0]
    mixed_groups = jnp.einsum(
        "tgc,gcd->tgd",
        pool_diff.reshape(length, groups_here, GROUP_CH),
        pool_mix,
        preferred_element_type=jnp.float32,
    )
    pool_out = (mixed_groups.reshape(length, pool_width) * pool_scale).astype(jnp.bfloat16)
    contract = (((0,), (1,)), ((), ()))
    mixed = summed_on_arrival(
        lax.dot_general(w_out_pool, pool_out, contract, preferred_element_type=jnp.float32)
        + lax.dot_general(w_out_rec, rec_out, contract, preferred_element_type=jnp.float32),
        "tp",
        0,
    ).T
    resid = ALPHA * features.astype(jnp.float32) + mixed
    row_total, squares = (
        total_of_pieces(jnp.sum(resid, axis=1), "tp"),
        total_of_pieces(jnp.sum(resid * resid, axis=1), "tp"),
    )
    row_mean = (row_total / D)[:, None]
    row_var = (squares / D)[:, None] - row_mean * row_mean
    normed = (resid - row_mean) * lax.rsqrt(row_var + EPS_NORM) * norm_gain + norm_bias
    return normed.astype(jnp.bfloat16)[None]


def solution(mesh):
    torus = Mesh(
        mesh.devices.reshape(4, 4, mesh.shape["fs"], mesh.shape["tp"]), ("sp_0", "sp_1", "fs", "tp")
    )
    return jax.shard_map(
        local,
        mesh=torus,
        in_specs=(
            P("fs", SP, "tp"),
            P(None, "tp"),
            P(None, "tp"),
            P(None, "tp"),
            P(None, "tp"),
            P(None, "tp"),
            P("tp", None, None),
            P("tp"),
            P("tp"),
            P(SP, "tp"),
            P(),
            P("tp", None),
            P("tp", None),
            P("tp"),
            P("tp"),
        ),
        out_specs=P("fs", SP, "tp"),
        check_vma=False,
    )
```

profile of v0, /device:TPU:1, one launch (start us, length us, event | category | flops | bytes accessed | tf_op | source)
XLA Modules:
  0.0 219.5 jit_solution(1167471921932692626)
XLA Ops:
  7.7 1.9 copy.110
  15.9 13.1 %all-gather.9.cloned.1.call-done = bf16[1,1024,2048]{2,1,0:T(8,128)(2,1)} async-done(((bf16[1,1024,1024]{2,1,0:T(8,128)(2,1)}), bf16[1,1024,2048]{2,1,0:T(8,128)(2,1)}) %all-gather.9.cloned.1.call-update) | async-done | bytes 4194320 | tf_op jit(solution)/shard_map/all_gather | solution.py:101
  29.0 5.2 %fusion.47 = bf16[1024,512]{1,0:T(8,128)(2,1)S(1)} fusion(bf16[2048,512]{1,0:T(8,128)(2,1)} %param.18, bf16[1,1024,2048]{2,1,0:T(8,128)(2,1)} %all-gather.9.cloned.1.call-done), kind=kOutput, calls=%fused_computation.83 | convolution fusion | flops 2148007936 | bytes 7340032 | tf_op jit(solution)/shard_map/dot_general | solution.py:103
  34.2 1.0 copy-done.6
  35.2 6.2 %fusion.44 = bf16[1024,512]{1,0:T(8,128)(2,1)} fusion(bf16[2048,512]{1,0:T(8,128)(2,1)} %param.21, bf16[1,1024,2048]{2,1,0:T(8,128)(2,1)} %all-gather.9.cloned.1.call-done), kind=kOutput, calls=%fused_computation.82 | convolution fusion | flops 2148007936 | bytes 7340032 | tf_op jit(solution)/shard_map/dot_general | solution.py:103
  41.4 1.3 reshape.465
  42.7 8.2 %broadcast_subtract_fusion = (f32[1024,512]{1,0:T(8,128)}, f32[1024,512]{1,0:T(8,128)}) fusion(bf16[2048,512]{1,0:T(8,128)(2,1)} %param.20, bf16[1,1024,2048]{2,1,0:T(8,128)(2,1)} %all-gather.9.cloned.1.call-done, f32[512]{0:T(512)S(1)} %broadcast_subtract_fusion.1, f32[512]{0:T(512)S(1)} %copy-done.18), kind=kOutput, calls=%fused_computation.92 | convolution fusion | flops 2151677952 | bytes 10489856 | tf_op jit(solution)/shard_map/dot_general | solution.py:103
  51.0 2.9 %copy.78 = f32[8,128,512]{1,2,0:T(8,128)} copy(f32[8,128,512]{2,1,0:T(8,128)} %bitcast.273) | data formatting | bytes 4194304 | tf_op jit(solution)/shard_map/reshape | solution.py:126
  53.9 2.9 %copy.76 = f32[8,128,512]{1,0,2:T(8,128)} copy(f32[8,128,512]{2,1,0:T(8,128)} %bitcast.272) | data formatting | bytes 4194304 | tf_op jit(solution)/shard_map/reshape | solution.py:114
  56.8 2.4 %bitcast_add_fusion.2 = bf16[8,128,512]{1,0,2:T(8,128)(2,1)S(1)} fusion(f32[8,128,512]{1,0,2:T(8,128)} %copy.76, f32[64,8,8,128]{3,2,1,0:T(8,128)} %copy.110), kind=kLoop, calls=%fused_computation.30 | loop fusion | flops 1048576 | bytes 5242880 | tf_op jit(solution)/shard_map/add | solution.py:114
  59.7 1.2 slice_reduce_fusion
  62.0 1.8 fusion.68
  63.8 15.4 %while.17 = (s32[]{:T(128)}, f32[4,128,128]{2,1,0:T(8,128)S(1)}, f32[512]{0:T(512)S(1)}, bf16[8,4,128,128]{3,2,1,0:T(8,128)(2,1)}, f32[8,512]{1,0:T(8,128)S(1)},...) while((s32[]{:T(128)}, f32[4,128,128]{2,1,0:T(8,128)S(1)}, ...), condition=%wide.region_1.2_spmd.clone, body=%wide.region_0.1_spmd.clone.sunk | while | flops 263171 | bytes 1200257 | solution.py:155
  64.5 1.1 bitcast_add_fusion.9
  66.5 1.1 bitcast_add_fusion.9
  68.4 1.1 bitcast_add_fusion.9
  70.3 1.1 bitcast_add_fusion.9
  72.2 1.1 bitcast_add_fusion.9
  74.2 1.1 bitcast_add_fusion.9
  76.1 1.1 bitcast_add_fusion.9
  78.0 1.1 bitcast_add_fusion.9
  79.2 11.5 %all-gather.5 = bf16[4,577,128]{2,1,0:T(8,128)(2,1)S(1)} all-gather(bf16[1,577,128]{2,1,0:T(8,128)(2,1)S(1)} %maximum_bitcast_fusion), channel_id=3, replica_groups=mesh['sp_0'=4,'sp_1'=4,'fs'=4,'tp'=2] {'sp_1'}, dimensions={0}, use_global_device_ids=true | all-gather | bytes 738560 | tf_op jit(solution)/shard_map/all_gather | solution.py:32
  97.9 11.0 %all-gather.6 = bf16[4,577,128]{2,1,0:T(8,128)(2,1)S(1)} all-gather(bf16[1,577,128]{2,1,0:T(8,128)(2,1)S(1)} %maximum_bitcast_fusion.1), channel_id=4, replica_groups=mesh['sp_0'=4,'sp_1'=4,'fs'=4,'tp'=2] {'sp_0'}, dimensions={0}, use_global_device_ids=true | all-gather | bytes 738560 | tf_op jit(solution)/shard_map/all_gather | solution.py:32
  111.4 0.9 slice_convert_fusion.3
  112.4 5.5 %convert_multiply_fusion.1 = f32[1024,512]{1,0:T(8,128)} fusion(bf16[2048,512]{1,0:T(8,128)(2,1)} %param.19, bf16[1,1024,2048]{2,1,0:T(8,128)(2,1)S(1)} %copy-done.38), kind=kOutput, calls=%fused_computation.21 | convolution fusion | flops 2150629376 | bytes 8388608 | tf_op jit(solution)/shard_map/dot_general | solution.py:103
  117.9 2.9 %copy.83 = f32[8,128,512]{1,2,0:T(8,128)} copy(f32[8,128,512]{2,1,0:T(8,128)} %bitcast.274) | data formatting | bytes 4194304 | tf_op jit(solution)/shard_map/reshape | solution.py:125
  120.8 6.8 %convert_multiply_fusion = f32[1024,512]{1,0:T(8,128)} fusion(bf16[2048,512]{1,0:T(8,128)(2,1)} %param.22, bf16[1,1024,2048]{2,1,0:T(8,128)(2,1)} %all-gather.9.cloned.1.call-done), kind=kOutput, calls=%fused_computation.19 | convolution fusion | flops 2150629376 | bytes 8388608 | tf_op jit(solution)/shard_map/dot_general | solution.py:103
  127.6 2.9 %copy.105 = f32[1024,512]{0,1:T(8,128)} copy(f32[1024,512]{1,0:T(8,128)} %convert_multiply_fusion) | data formatting | bytes 4194304 | tf_op jit(solution)/shard_map/reshape | solution.py:191
  130.5 4.1 %exponential_multiply_fusion = (bf16[8,128,512]{1,2,0:T(8,128)(2,1)S(1)}, bf16[8,128,512]{1,2,0:T(8,128)(2,1)S(1)}, bf16[8,128,512]{1,2,0:T(8,128)(2,1)}) fusion(f32[8,128,512]{1,2,0:T(8,128)} %copy.83, f32[8,128,512]{1,2,0:T(8,128)} %copy-done.1, f32[8,512]{1,0:T(8,128)S(1)} %get-tuple-element.48, f32[8,128,512]{1,2,0:T(8,128)} %copy.78), kind=kLoop, calls=%fused_computation.72 | loop fusion | flops 4194304 | bytes 9453568 | tf_op jit(solution)/shard_map/mul | solution.py:159
  134.6 1.6 copy.91
  136.3 2.3 %reshape.477 = bf16[1024,4,128]{0,2,1:T(8,128)(2,1)} reshape(bf16[8,128,512]{1,0,2:T(8,128)(2,1)} %copy.91) | data formatting | bytes 2097152 | tf_op jit(solution)/shard_map/reshape | solution.py:159
  141.8 1.5 select_convert_fusion
  144.1 3.1 %fusion.148 = f32[8,4,128,128]{2,3,1,0:T(8,128)} fusion(bf16[8,4,128,128]{3,2,1,0:T(8,128)(2,1)} %get-tuple-element.47, bf16[8,128,4,128]{1,3,2,0:T(8,128)(2,1)S(1)} %bitcast.263), kind=kOutput, calls=%fused_computation.232 | convolution fusion | flops 134217728 | bytes 4194304 | tf_op jit(solution)/shard_map/bthd,bhde->bthe/dot_general | solution.py:157
  147.1 4.4 %add_bitcast_fusion = f32[8,128,4,128]{3,1,2,0:T(8,128)} fusion(f32[8,4,128,128]{2,3,1,0:T(8,128)} %fusion.148, bf16[8,128,4,128]{1,3,2,0:T(8,128)(2,1)S(1)} %bitcast.264, bf16[8,128,4,128]{1,3,2,0:T(8,128)(2,1)} %bitcast.269, f32[128,128]{1,0:T(8,128)} %fusion.114, bf16[8,128,4,128]{3,2,1,0:T(4,128)(2,1)} %copy-done.3), kind=kOutput, calls=%fused_computation.73 | convolution fusion | flops 270008320 | bytes 7405568 | tf_op jit(solution)/shard_map/bhts,bshe->bthe/dot_general | solution.py:131
  151.5 3.1 %copy.89 = f32[8,128,4,128]{3,1,0,2:T(8,128)} copy(f32[8,128,4,128]{3,1,2,0:T(8,128)} %add_bitcast_fusion) | data formatting | bytes 4194304 | tf_op jit(solution)/shard_map/add | solution.py:158
  154.7 3.0 %copy.94 = f32[1024,4,128]{0,2,1:T(8,128)} copy(f32[1024,4,128]{2,0,1:T(8,128)} %bitcast.266) | data formatting | bytes 4194304 | tf_op jit(solution)/shard_map/reshape | solution.py:158
  157.6 3.3 %multiply_reduce_fusion.1 = (f32[1024,4]{0,1:T(4,128)S(1)}, f32[1024,4,128]{0,2,1:T(8,128)S(1)}) fusion(f32[1024,4,128]{0,2,1:T(8,128)} %copy.94, bf16[1024,4,128]{0,2,1:T(8,128)(2,1)S(1)} %copy-done.8, bf16[4,128,128]{2,1,0:T(8,128)(2,1)} %bitcast.283, bf16[4,128,128]{2,1,0:T(8,128)(2,1)} %bitcast.282, f32[4,128,128]{2,1,0:T(8,128)} %bitcast.278, ...), kind=kOutput, calls=%fused_computation.71 | convolution fusion | flops 137621504 | bytes 6850568 | tf_op jit(solution)/shard_map/thd,hde->the/dot_general | solution.py:185
  161.8 6.2 %fusion.37 = bf16[1024,512]{1,0:T(8,128)(2,1)S(1)} fusion(bf16[1024,512]{1,0:T(8,128)(2,1)S(1)} %copy-done.7, f32[1039,512]{1,0:T(8,128)S(1)} %maximum_convert_fusion, f32[512]{0:T(512)S(1)} %copy-done.14, f32[1024]{0:T(1024)S(1)} %copy-done.13, pred[512]{0:T(512)(128)(4,1)S(1)} %copy-done.34, pred[512]{0:T(512)(128)(4,1)S(1)} %copy-done.35, ...), kind=kLoop, calls=%fused_computation.79 | loop fusion | flops 18874368 | bytes 35665920 | tf_op jit(solution)/shard_map/convert_element_type | solution.py:205
  168.9 2.4 %fusion.147 = f32[1024,2048]{1,0:T(8,128)S(1)} fusion(bf16[1024,512]{0,1:T(8,128)(2,1)S(1)} %fusion.34, bf16[512,2048]{1,0:T(8,128)(2,1)S(1)} %copy-done), kind=kOutput, calls=%fused_computation.231 | convolution fusion | flops 2147483648 | bytes 11534336 | tf_op jit(solution)/shard_map/dot_general | solution.py:216
  171.9 1.0 copy-done.10
  172.9 2.4 %convolution_add_fusion = f32[1024,2048]{1,0:T(8,128)S(1)} fusion(f32[1024,2048]{1,0:T(8,128)S(1)} %fusion.147, bf16[1024,512]{0,1:T(8,128)(2,1)S(1)} %bitcast.268, bf16[512,2048]{1,0:T(8,128)(2,1)S(1)} %copy-done.10), kind=kOutput, calls=%fused_computation.18 | convolution fusion | flops 2149580800 | bytes 19922944 | tf_op jit(solution)/shard_map/dot_general | solution.py:217
  175.4 1.7 copy.126
  177.0 17.0 %all_to_all.5 = f32[2,1024,1024]{1,2,0:T(8,128)} all-to-all(f32[2,1024,1024]{1,2,0:T(8,128)S(1)} %bitcast.262), channel_id=1, replica_groups=mesh['sp_0'=4,'sp_1'=4,'fs'=4,'tp'=2] {'tp'}, dimensions={0} | all-to-all | bytes 16777216 | tf_op jit(solution)/shard_map/all_to_all | solution.py:72
  194.0 6.7 %reduce_sum.55 = f32[1024,1024]{0,1:T(8,128)} reduce(f32[2,1024,1024]{1,2,0:T(8,128)} %all_to_all.5, f32[]{:T(128)} %constant.50.clone.1), dimensions={0}, to_apply=%region_3.4 | reduce | flops 1048576 | bytes 12582916 | tf_op jit(solution)/shard_map/reduce_sum | solution.py:73
  200.7 3.8 %fusion.62 = (f32[1024]{0:T(1024)S(1)}, f32[1024]{0:T(1024)S(1)}) fusion(f32[1024,1024]{0,1:T(8,128)} %reduce_sum.55, bf16[1,1024,1024]{2,1,0:T(8,128)(2,1)} %param.17), kind=kLoop, calls=%fused_computation.86 | loop fusion | flops 6289408 | bytes 6299648 | tf_op jit(solution)/shard_map/reduce_sum | solution.py:223
  204.5 1.8 all-gather.3
  206.4 1.8 all-gather.4
  208.3 4.4 %fusion.16 = bf16[1,1024,1024]{2,1,0:T(8,128)(2,1)} fusion(f32[1024]{0:T(1024)S(1)} %copy-done.16, f32[1024]{0:T(1024)S(1)} %copy-done.17, f32[1024]{0:T(1024)S(1)} %get-tuple-element.119, f32[1024]{0:T(1024)S(1)} %get-tuple-element.118, f32[1024,1024]{0,1:T(8,128)} %reduce_sum.55, bf16[1,1024,1024]{2,1,0:T(8,128)(2,1)} %param.17), kind=kLoop, calls=%fused_computation.29 | loop fusion | flops 8388608 | bytes 8404992 | tf_op jit(solution)/shard_map/broadcast_in_dim | solution.py:229
  (161 shorter events, 23.5 us)
Async XLA Ops:
  6.5 162.3 %copy-start = (bf16[512,2048]{1,0:T(8,128)(2,1)S(1)}, bf16[512,2048]{1,0:T(8,128)(2,1)}, u32[]{:S(2)}) copy-start(bf16[512,2048]{1,0:T(8,128)(2,1)} %param.28) | copy-start | bytes 6291460
  6.5 0.9 copy-start.12
  6.5 22.5 %all-gather.9.cloned.1.call-start = ((), (), s32[]{:S(2)}) async-start(), calls=%async_computation.1 | async-start | bytes 6291456 | tf_op jit(solution)/shard_map/all_gather | solution.py:101
  7.7 8.3 %copy-start.18 = (f32[512]{0:T(512)S(1)}, f32[512]{0:T(512)}, u32[]{:S(2)}) copy-start(f32[512]{0:T(512)} %param.25) | copy-start | bytes 6148
  34.2 1.0 copy-start.6
  42.7 19.2 %copy-start.3 = (bf16[8,128,4,128]{3,2,1,0:T(4,128)(2,1)}, bf16[8,128,4,128]{3,2,1,0:T(4,128)(2,1)S(1)}, u32[]{:S(2)}) copy-start(bf16[8,128,4,128]{3,2,1,0:T(4,128)(2,1)S(1)} %reshape.465) | copy-start | bytes 3145732
  59.2 2.0 copy-start.2
  59.7 2.3 %copy-start.1 = (f32[8,128,512]{1,2,0:T(8,128)}, f32[8,128,512]{1,2,0:T(8,128)S(1)}, u32[]{:S(2)}) copy-start(f32[8,128,512]{1,2,0:T(8,128)S(1)} %fusion.38) | copy-start | bytes 6291460
  63.8 15.4 %copy-start.20 = (bf16[1,128]{1,0:T(2,128)(2,1)S(1)}, bf16[1,128]{1,0:T(2,128)(2,1)}, u32[]{:S(2)}) copy-start(bf16[1,128]{1,0:T(2,128)(2,1)} %constant.36.clone.1) | copy-start | bytes 772
  90.7 20.8 %copy-start.5 = (bf16[4,577,128]{2,1,0:T(8,128)(2,1)}, bf16[4,577,128]{2,1,0:T(8,128)(2,1)S(1)}, u32[]{:S(2)}) copy-start(bf16[4,577,128]{2,1,0:T(8,128)(2,1)S(1)} %all-gather.5) | copy-start | bytes 1772548
  97.5 14.8 %copy-start.38 = (bf16[1,1024,2048]{2,1,0:T(8,128)(2,1)S(1)}, bf16[1,1024,2048]{2,1,0:T(8,128)(2,1)}, u32[]{:S(2)}) copy-start(bf16[1,1024,2048]{2,1,0:T(8,128)(2,1)} %all-gather.9.cloned.1.call-done) | copy-start | bytes 12582916
  108.9 1.8 copy-start.9
  134.6 4.0 %copy-start.15 = (bf16[4,1,128]{2,1,0:T(2,128)(2,1)S(1)}, bf16[4,1,128]{2,1,0:T(2,128)(2,1)}, u32[]{:S(2)}) copy-start(bf16[4,1,128]{2,1,0:T(2,128)(2,1)} %slice.279) | copy-start | bytes 3076
  154.7 3.0 %copy-start.8 = (bf16[1024,4,128]{0,2,1:T(8,128)(2,1)S(1)}, bf16[1024,4,128]{0,2,1:T(8,128)(2,1)}, u32[]{:S(2)}) copy-start(bf16[1024,4,128]{0,2,1:T(8,128)(2,1)} %reshape.477) | copy-start | bytes 3145732
  157.6 3.5 %copy-start.7 = (bf16[1024,512]{1,0:T(8,128)(2,1)S(1)}, bf16[1024,512]{1,0:T(8,128)(2,1)}, u32[]{:S(2)}) copy-start(bf16[1024,512]{1,0:T(8,128)(2,1)} %copy-done.6) | copy-start | bytes 3145732
  161.0 0.7 copy-start.13
  161.0 0.7 copy-start.14
  161.0 0.7 copy-start.22
  161.0 0.7 copy-start.23
  161.0 0.7 copy-start.24
  161.0 0.7 copy-start.25
  161.0 0.6 copy-start.26
  161.0 0.6 copy-start.27
  161.0 0.6 copy-start.28
  161.1 0.6 copy-start.29
  161.1 0.7 copy-start.30
  161.1 0.7 copy-start.31
  161.1 0.7 copy-start.32
  161.1 0.7 copy-start.33
  161.1 0.7 copy-start.34
  161.1 0.7 copy-start.35
  161.1 0.7 copy-start.36
  161.1 0.7 copy-start.37
  161.8 6.2 %copy-start.11 = (bf16[2,256,256]{2,1,0:T(8,128)(2,1)S(1)}, bf16[2,256,256]{2,1,0:T(8,128)(2,1)}, u32[]{:S(2)}) copy-start(bf16[2,256,256]{2,1,0:T(8,128)(2,1)} %param.23) | copy-start | bytes 786436
  168.0 0.7 copy-start.19
  168.8 2.4 %copy-start.4 = (f32[1024,512]{0,1:T(8,128)S(1)}, f32[1024,512]{0,1:T(8,128)}, u32[]{:S(2)}) copy-start(f32[1024,512]{0,1:T(8,128)} %copy.105) | copy-start | bytes 6291460
  168.9 2.4 %copy-start.21 = (f32[128]{0:T(128)S(1)}, f32[128]{0:T(128)}, u32[]{:S(2)}) copy-start(f32[128]{0:T(128)} %param.27) | copy-start | bytes 1540
  171.3 1.6 copy-start.10
  200.7 7.6 %copy-start.16 = (f32[1024]{0:T(1024)S(1)}, f32[1024]{0:T(1024)}, u32[]{:S(2)}) copy-start(f32[1024]{0:T(1024)} %param.31) | copy-start | bytes 12292
  200.7 7.6 %copy-start.17 = (f32[1024]{0:T(1024)S(1)}, f32[1024]{0:T(1024)}, u32[]{:S(2)}) copy-start(f32[1024]{0:T(1024)} %param.30) | copy-start | bytes 12292
Sparse Core Ops, SparseCore 0:
  9.0 19.9 all-gather.8
where the time goes:
time: 221 us; the launch traced here: 220 us
  other arithmetic  55.6 us (25%)
  matrix products  50.2 us (23%)
  blocking collectives  43.1 us (20%)
  local copies, waits for them, and re-layouts  35 us (16%)
  between operations  21.6 us (10%)
  waiting for transfers between devices  13.8 us (6%)
    dot_general x5, matrix products, local(): jnp.dot(column_piece, weight, preferred_element_type=jnp.float32)  31.9 us
    all_gather x2, blocking collectives, gathered_once(): both, at, found = (lax.all_gather(jnp.concatenate(lines), axis), 0, {})  22.4 us
    all_to_all x1, blocking collectives, summed_on_arrival(): pieces = lax.all_to_all(split_up(x, dim, devices), axis, 0, 0, tiled=True)  17 us
    all_gather x1, waiting for transfers between devices, local(): column_piece = lax.all_gather(features, 'tp', axis=1, tiled=True)  13.1 us
    add x8, other arithmetic, block_step(): jnp.exp(end_blk).reshape(heads_here, DK)[:, :, None] * state + term_blk  8.93 us
    reduce_sum x1, other arithmetic, summed_on_arrival(): return jnp.sum(pieces, axis=0)  6.73 us
    convert_element_type x1, other arithmetic, local(): (window_sum / counts - pooled.astype(jnp.float32)).astype(jnp.bfloat16)  6.16 us
    dynamic_update_slice x8, other arithmetic, local(): lax.scan(block_step, start_carry, (log_end, own_terms))  5.44 us
  transfers between devices with their start and end apart: 1, of which 1 were waited for; matrix products, arithmetic and copies ran while one was open for 4% of the time, Pallas kernels for 0%

commit v1 on v0

--- a/solution.py
+++ b/solution.py
@@ -98,7 +98,8 @@
     features = stream[0]
     length = features.shape[0]
     weights = (w_pool_in, w_query, w_forget, w_value, w_outgate)
-    column_piece = lax.all_gather(features, "tp", axis=1, tiled=True)
+    copies = jnp.concatenate([features] * lax.axis_size("tp"), axis=1)
+    column_piece = lax.all_to_all(copies, "tp", 1, 1, tiled=True)
     projected = tuple(
         (jnp.dot(column_piece, weight, preferred_element_type=jnp.float32) for weight in weights)
     )

time: 221 us -> 212 us (0.959)
  waiting for transfers between devices: 13.8 us -> 0.01 us
  between operations: 21.6 us -> 8.51 us
  starting transfers between devices: 0.01 us -> 7.13 us
  other arithmetic: 55.6 us -> 60.3 us
  local copies, waits for them, and re-layouts: 35 us -> 39.1 us
    all_gather x1 -> x0, waiting for transfers between devices: 13.1 us -> none  [local(): column_piece = lax.all_gather(features, 'tp', axis=1, tiled=True)]
    all_to_all x0 -> x1, starting transfers between devices: none -> 7.13 us  [local(): column_piece = lax.all_to_all(copies, 'tp', 1, 1, tiled=True)]
    concatenate x0 -> x1, other arithmetic: none -> 4.64 us  [local(): copies = jnp.concatenate([features] * lax.axis_size('tp'), axis=1)]
    unnamed x81 -> x80, local copies, waits for them, and re-layouts: 4.8 us -> 8.79 us
  transfers between devices with their start and end apart: 1 -> 1, of which waited for: 1 -> 0; matrix products, arithmetic and copies ran while one was open for 4% -> 4% of each run, Pallas kernels for 0% -> 0%
where the time goes in v1:
time: 212 us; the launch traced here: 211 us
  other arithmetic  60.3 us (28%)
  matrix products  51.7 us (24%)
  blocking collectives  43.9 us (21%)
  local copies, waits for them, and re-layouts  39.1 us (18%)
  between operations  8.51 us (4%)
  starting transfers between devices  7.13 us (3%)
    dot_general x5, matrix products, local(): jnp.dot(column_piece, weight, preferred_element_type=jnp.float32)  33.4 us
    all_gather x2, blocking collectives, gathered_once(): both, at, found = (lax.all_gather(jnp.concatenate(lines), axis), 0, {})  23.1 us
    all_to_all x1, blocking collectives, summed_on_arrival(): pieces = lax.all_to_all(split_up(x, dim, devices), axis, 0, 0, tiled=True)  17.1 us
    add x8, other arithmetic, block_step(): jnp.exp(end_blk).reshape(heads_here, DK)[:, :, None] * state + term_blk  8.93 us
    unnamed x80, local copies, waits for them, and re-layouts  8.79 us
    all_to_all x1, starting transfers between devices, local(): column_piece = lax.all_to_all(copies, 'tp', 1, 1, tiled=True)  7.13 us
    reduce_sum x1, other arithmetic, summed_on_arrival(): return jnp.sum(pieces, axis=0)  6.74 us
    convert_element_type x1, other arithmetic, local(): (window_sum / counts - pooled.astype(jnp.float32)).astype(jnp.bfloat16)  6.13 us
  transfers between devices with their start and end apart: 1, of which 0 were waited for; matrix products, arithmetic and copies ran while one was open for 4% of the time, Pallas kernels for 0%

profile of v1, /device:TPU:1, one launch (start us, length us, event | category | flops | bytes accessed | tf_op | source)
XLA Modules:
  0.0 211.0 jit_solution(13036888244263344273)
XLA Ops:
  0.0 4.1 %copy.78 = bf16[1,1024,1024]{1,2,0:T(8,128)(2,1)} copy(bf16[1,1024,1024]{2,1,0:T(8,128)(2,1)} %param.17) | data formatting | bytes 4194304 | tf_op args[0]
  4.1 4.6 %pad_maximum_fusion = bf16[1024,2,1024]{0,2,1:T(8,128)(2,1)} fusion(bf16[1024,1,1024]{0,2,1:T(8,128)(2,1)} %bitcast.243), kind=kLoop, calls=%fused_computation.5 | loop fusion | flops 2097152 | bytes 6291456 | tf_op jit(solution)/shard_map/concatenate | solution.py:101
  8.7 7.1 %all-to-all-start = ((bf16[1024,2,1024]{0,2,1:T(8,128)(2,1)}), bf16[1024,2,1024]{0,2,1:T(8,128)(2,1)}, u32[]{:S(2)}, u32[]{:S(2)}) async-start(bf16[1024,2,1024]{0,2,1:T(8,128)(2,1)} %pad_maximum_fusion), calls=%async_computation | async-start | bytes 8388608 | tf_op jit(solution)/shard_map/all_to_all | solution.py:102
  22.0 1.8 copy.113
  23.8 5.2 %convolution_convert_fusion.2 = bf16[1024,512]{1,0:T(8,128)(2,1)S(1)} fusion(bf16[1024,2048]{0,1:T(8,128)(2,1)} %bitcast.3, bf16[2048,512]{1,0:T(8,128)(2,1)} %param.18), kind=kOutput, calls=%fused_computation.74 | convolution fusion | flops 2148007936 | bytes 7340032 | tf_op jit(solution)/shard_map/dot_general | solution.py:104
  30.0 6.2 %convolution_convert_fusion.3 = bf16[1024,512]{1,0:T(8,128)(2,1)} fusion(bf16[1024,2048]{0,1:T(8,128)(2,1)} %bitcast.3, bf16[2048,512]{1,0:T(8,128)(2,1)} %param.21), kind=kOutput, calls=%fused_computation.75 | convolution fusion | flops 2148007936 | bytes 7340032 | tf_op jit(solution)/shard_map/dot_general | solution.py:104
  36.2 1.3 reshape.474
  37.6 8.3 %broadcast_subtract_fusion = (f32[1024,512]{1,0:T(8,128)}, f32[1024,512]{1,0:T(8,128)}) fusion(bf16[1024,2048]{0,1:T(8,128)(2,1)} %bitcast.3, bf16[2048,512]{1,0:T(8,128)(2,1)} %param.20, f32[512]{0:T(512)S(1)} %broadcast_subtract_fusion.1, f32[512]{0:T(512)S(1)} %copy-done.18), kind=kOutput, calls=%fused_computation.83 | convolution fusion | flops 2151677952 | bytes 10489856 | tf_op jit(solution)/shard_map/dot_general | solution.py:104
  45.9 3.0 %copy.81 = f32[8,128,512]{1,2,0:T(8,128)} copy(f32[8,128,512]{2,1,0:T(8,128)} %bitcast.252) | data formatting | bytes 4194304 | tf_op jit(solution)/shard_map/reshape | solution.py:127
  48.9 2.9 %copy.79 = f32[8,128,512]{1,0,2:T(8,128)} copy(f32[8,128,512]{2,1,0:T(8,128)} %bitcast.251) | data formatting | bytes 4194304 | tf_op jit(solution)/shard_map/reshape | solution.py:115
  51.7 2.4 %bitcast_add_fusion.2 = bf16[8,128,512]{1,0,2:T(8,128)(2,1)S(1)} fusion(f32[8,128,512]{1,0,2:T(8,128)} %copy.79, f32[64,8,8,128]{3,2,1,0:T(8,128)} %copy.113), kind=kLoop, calls=%fused_computation.21 | loop fusion | flops 1048576 | bytes 5242880 | tf_op jit(solution)/shard_map/add | solution.py:115
  54.6 1.2 slice_reduce_fusion
  56.9 1.8 fusion.37
  58.7 15.4 %while.17 = (s32[]{:T(128)}, f32[4,128,128]{2,1,0:T(8,128)S(1)}, f32[512]{0:T(512)S(1)}, bf16[8,4,128,128]{3,2,1,0:T(8,128)(2,1)}, f32[8,512]{1,0:T(8,128)S(1)},...) while((s32[]{:T(128)}, f32[4,128,128]{2,1,0:T(8,128)S(1)}, ...), condition=%wide.region_1.2_spmd.clone, body=%wide.region_0.1_spmd.clone.sunk | while | flops 263171 | bytes 1200257 | solution.py:156
  59.5 1.1 bitcast_add_fusion.9
  61.4 1.1 bitcast_add_fusion.9
  63.3 1.1 bitcast_add_fusion.9
  65.3 1.1 bitcast_add_fusion.9
  67.2 1.1 bitcast_add_fusion.9
  69.1 1.1 bitcast_add_fusion.9
  71.1 1.1 bitcast_add_fusion.9
  73.0 1.1 bitcast_add_fusion.9
  74.2 11.4 %all-gather.4 = bf16[4,577,128]{2,1,0:T(8,128)(2,1)S(1)} all-gather(bf16[1,577,128]{2,1,0:T(8,128)(2,1)S(1)} %maximum_bitcast_fusion), channel_id=2, replica_groups=mesh['sp_0'=4,'sp_1'=4,'fs'=4,'tp'=2] {'sp_1'}, dimensions={0}, use_global_device_ids=true | all-gather | bytes 738560 | tf_op jit(solution)/shard_map/all_gather | solution.py:32
  93.2 11.7 %all-gather.5 = bf16[4,577,128]{2,1,0:T(8,128)(2,1)S(1)} all-gather(bf16[1,577,128]{2,1,0:T(8,128)(2,1)S(1)} %maximum_bitcast_fusion.1), channel_id=3, replica_groups=mesh['sp_0'=4,'sp_1'=4,'fs'=4,'tp'=2] {'sp_0'}, dimensions={0}, use_global_device_ids=true | all-gather | bytes 738560 | tf_op jit(solution)/shard_map/all_gather | solution.py:32
  109.1 6.9 %convert_multiply_fusion = f32[1024,512]{1,0:T(8,128)} fusion(bf16[1024,2048]{0,1:T(8,128)(2,1)} %bitcast.3, bf16[2048,512]{1,0:T(8,128)(2,1)} %param.22), kind=kOutput, calls=%fused_computation.10 | convolution fusion | flops 2150629376 | bytes 8388608 | tf_op jit(solution)/shard_map/dot_general | solution.py:104
  116.0 2.9 %copy.108 = f32[1024,512]{0,1:T(8,128)} copy(f32[1024,512]{1,0:T(8,128)} %convert_multiply_fusion) | data formatting | bytes 4194304 | tf_op jit(solution)/shard_map/reshape | solution.py:192
  118.9 6.8 %convert_multiply_fusion.1 = f32[1024,512]{1,0:T(8,128)} fusion(bf16[1024,2048]{0,1:T(8,128)(2,1)} %bitcast.3, bf16[2048,512]{1,0:T(8,128)(2,1)} %param.19), kind=kOutput, calls=%fused_computation.12 | convolution fusion | flops 2150629376 | bytes 8388608 | tf_op jit(solution)/shard_map/dot_general | solution.py:104
  125.7 2.9 %copy.86 = f32[8,128,512]{1,2,0:T(8,128)} copy(f32[8,128,512]{2,1,0:T(8,128)} %bitcast.253) | data formatting | bytes 4194304 | tf_op jit(solution)/shard_map/reshape | solution.py:126
  128.7 4.1 %exponential_multiply_fusion = (bf16[8,128,512]{1,2,0:T(8,128)(2,1)S(1)}, bf16[8,128,512]{1,2,0:T(8,128)(2,1)S(1)}, bf16[8,128,512]{1,2,0:T(8,128)(2,1)}) fusion(f32[8,128,512]{1,2,0:T(8,128)} %copy.86, f32[8,128,512]{1,2,0:T(8,128)} %copy-done.1, f32[8,512]{1,0:T(8,128)S(1)} %get-tuple-element.48, f32[8,128,512]{1,2,0:T(8,128)} %copy.81), kind=kLoop, calls=%fused_computation.63 | loop fusion | flops 4194304 | bytes 9453568 | tf_op jit(solution)/shard_map/mul | solution.py:160
  132.8 1.6 copy.94
  134.5 2.3 %reshape.486 = bf16[1024,4,128]{0,2,1:T(8,128)(2,1)} reshape(bf16[8,128,512]{1,0,2:T(8,128)(2,1)} %copy.94) | data formatting | bytes 2097152 | tf_op jit(solution)/shard_map/reshape | solution.py:160
  139.9 1.5 select_convert_fusion
  142.2 3.1 %fusion.117 = f32[8,4,128,128]{2,3,1,0:T(8,128)} fusion(bf16[8,4,128,128]{3,2,1,0:T(8,128)(2,1)} %get-tuple-element.47, bf16[8,128,4,128]{1,3,2,0:T(8,128)(2,1)S(1)} %bitcast.241), kind=kOutput, calls=%fused_computation.223 | convolution fusion | flops 134217728 | bytes 4194304 | tf_op jit(solution)/shard_map/bthd,bhde->bthe/dot_general | solution.py:158
  145.2 4.4 %add_bitcast_fusion = f32[8,128,4,128]{3,1,2,0:T(8,128)} fusion(f32[8,4,128,128]{2,3,1,0:T(8,128)} %fusion.117, bf16[8,128,4,128]{1,3,2,0:T(8,128)(2,1)S(1)} %bitcast.242, bf16[8,128,4,128]{1,3,2,0:T(8,128)(2,1)} %bitcast.248, f32[128,128]{1,0:T(8,128)} %fusion.83, bf16[8,128,4,128]{3,2,1,0:T(4,128)(2,1)} %copy-done.3), kind=kOutput, calls=%fused_computation.64 | convolution fusion | flops 270008320 | bytes 7405568 | tf_op jit(solution)/shard_map/bhts,bshe->bthe/dot_general | solution.py:132
  149.6 3.2 %copy.92 = f32[8,128,4,128]{3,1,0,2:T(8,128)} copy(f32[8,128,4,128]{3,1,2,0:T(8,128)} %add_bitcast_fusion) | data formatting | bytes 4194304 | tf_op jit(solution)/shard_map/add | solution.py:159
  152.8 3.0 %copy.97 = f32[1024,4,128]{0,2,1:T(8,128)} copy(f32[1024,4,128]{2,0,1:T(8,128)} %bitcast.245) | data formatting | bytes 4194304 | tf_op jit(solution)/shard_map/reshape | solution.py:159
  155.8 3.3 %multiply_reduce_fusion.1 = (f32[1024,4]{0,1:T(4,128)S(1)}, f32[1024,4,128]{0,2,1:T(8,128)S(1)}) fusion(f32[1024,4,128]{0,2,1:T(8,128)} %copy.97, bf16[1024,4,128]{0,2,1:T(8,128)(2,1)S(1)} %copy-done.8, bf16[4,128,128]{2,1,0:T(8,128)(2,1)} %bitcast.262, bf16[4,128,128]{2,1,0:T(8,128)(2,1)} %bitcast.261, f32[4,128,128]{2,1,0:T(8,128)} %bitcast.257, ...), kind=kOutput, calls=%fused_computation.62 | convolution fusion | flops 137621504 | bytes 6850568 | tf_op jit(solution)/shard_map/thd,hde->the/dot_general | solution.py:186
  160.0 6.1 %fusion.27 = bf16[1024,512]{1,0:T(8,128)(2,1)S(1)} fusion(bf16[1024,512]{1,0:T(8,128)(2,1)S(1)} %copy-done.7, f32[1039,512]{1,0:T(8,128)S(1)} %maximum_convert_fusion, f32[512]{0:T(512)S(1)} %copy-done.14, f32[1024]{0:T(1024)S(1)} %copy-done.13, pred[512]{0:T(512)(128)(4,1)S(1)} %copy-done.34, pred[512]{0:T(512)(128)(4,1)S(1)} %copy-done.35, ...), kind=kLoop, calls=%fused_computation.70 | loop fusion | flops 18874368 | bytes 35665920 | tf_op jit(solution)/shard_map/convert_element_type | solution.py:206
  167.0 2.4 %fusion.116 = f32[1024,2048]{1,0:T(8,128)S(1)} fusion(bf16[1024,512]{0,1:T(8,128)(2,1)S(1)} %fusion.24, bf16[512,2048]{1,0:T(8,128)(2,1)S(1)} %copy-done), kind=kOutput, calls=%fused_computation.222 | convolution fusion | flops 2147483648 | bytes 11534336 | tf_op jit(solution)/shard_map/dot_general | solution.py:217
  170.1 1.0 copy-done.10
  171.0 2.4 %convolution_add_fusion = f32[1024,2048]{1,0:T(8,128)S(1)} fusion(f32[1024,2048]{1,0:T(8,128)S(1)} %fusion.116, bf16[1024,512]{0,1:T(8,128)(2,1)S(1)} %bitcast.247, bf16[512,2048]{1,0:T(8,128)(2,1)S(1)} %copy-done.10), kind=kOutput, calls=%fused_computation.9 | convolution fusion | flops 2149580800 | bytes 19922944 | tf_op jit(solution)/shard_map/dot_general | solution.py:218
  173.5 1.7 copy.129
  175.2 17.1 %all_to_all.14 = f32[2,1024,1024]{1,2,0:T(8,128)} all-to-all(f32[2,1024,1024]{1,2,0:T(8,128)S(1)} %bitcast.240), channel_id=1, replica_groups=mesh['sp_0'=4,'sp_1'=4,'fs'=4,'tp'=2] {'tp'}, dimensions={0} | all-to-all | bytes 16777216 | tf_op jit(solution)/shard_map/all_to_all | solution.py:72
  192.3 6.7 %reduce_sum.55 = f32[1024,1024]{0,1:T(8,128)} reduce(f32[2,1024,1024]{1,2,0:T(8,128)} %all_to_all.14, f32[]{:T(128)} %constant.50.clone.1), dimensions={0}, to_apply=%region_3.4 | reduce | flops 1048576 | bytes 12582916 | tf_op jit(solution)/shard_map/reduce_sum | solution.py:73
  199.0 3.8 %fusion.31 = (f32[1024]{0:T(1024)S(1)}, f32[1024]{0:T(1024)S(1)}) fusion(f32[1024,1024]{0,1:T(8,128)} %reduce_sum.55, bf16[1,1024,1024]{2,1,0:T(8,128)(2,1)} %param.17), kind=kLoop, calls=%fused_computation.77 | loop fusion | flops 6289408 | bytes 6299648 | tf_op jit(solution)/shard_map/reduce_sum | solution.py:224
  202.8 1.8 all-gather.2
  204.7 1.8 all-gather.3
  206.6 4.4 %fusion.6 = bf16[1,1024,1024]{2,1,0:T(8,128)(2,1)} fusion(f32[1024]{0:T(1024)S(1)} %copy-done.16, f32[1024]{0:T(1024)S(1)} %copy-done.17, f32[1024]{0:T(1024)S(1)} %get-tuple-element.119, f32[1024]{0:T(1024)S(1)} %get-tuple-element.118, f32[1024,1024]{0,1:T(8,128)} %reduce_sum.55, bf16[1,1024,1024]{2,1,0:T(8,128)(2,1)} %param.17), kind=kLoop, calls=%fused_computation.20 | loop fusion | flops 8388608 | bytes 8404992 | tf_op jit(solution)/shard_map/broadcast_in_dim | solution.py:230
  (160 shorter events, 24.8 us)
Async XLA Ops:
  0.0 167.0 %copy-start = (bf16[512,2048]{1,0:T(8,128)(2,1)S(1)}, bf16[512,2048]{1,0:T(8,128)(2,1)}, u32[]{:S(2)}) copy-start(bf16[512,2048]{1,0:T(8,128)(2,1)} %param.28) | copy-start | bytes 6291460
  8.7 13.0 %copy-start.18 = (f32[512]{0:T(512)S(1)}, f32[512]{0:T(512)}, u32[]{:S(2)}) copy-start(f32[512]{0:T(512)} %param.25) | copy-start | bytes 6148
  8.7 13.0 %copy-start.12 = (f32[1024,4]{0,1:T(4,128)S(1)}, f32[1024,4]{0,1:T(4,128)}, u32[]{:S(2)}) copy-start(f32[1024,4]{0,1:T(4,128)} %param.26) | copy-start | bytes 49156
  8.7 15.1 %all-to-all-start = ((bf16[1024,2,1024]{0,2,1:T(8,128)(2,1)}), bf16[1024,2,1024]{0,2,1:T(8,128)(2,1)}, u32[]{:S(2)}, u32[]{:S(2)}) async-start(bf16[1024,2,1024]{0,2,1:T(8,128)(2,1)} %pad_maximum_fusion), calls=%async_computation | async-start | bytes 8388608 | tf_op jit(solution)/shard_map/all_to_all | solution.py:102
  29.0 1.0 copy-start.6
  37.6 19.3 %copy-start.3 = (bf16[8,128,4,128]{3,2,1,0:T(4,128)(2,1)}, bf16[8,128,4,128]{3,2,1,0:T(4,128)(2,1)S(1)}, u32[]{:S(2)}) copy-start(bf16[8,128,4,128]{3,2,1,0:T(4,128)(2,1)S(1)} %reshape.474) | copy-start | bytes 3145732
  54.2 2.0 copy-start.2
  54.6 2.3 %copy-start.1 = (f32[8,128,512]{1,2,0:T(8,128)}, f32[8,128,512]{1,2,0:T(8,128)S(1)}, u32[]{:S(2)}) copy-start(f32[8,128,512]{1,2,0:T(8,128)S(1)} %fusion.28) | copy-start | bytes 6291460
  58.7 15.5 %copy-start.20 = (bf16[1,128]{1,0:T(2,128)(2,1)S(1)}, bf16[1,128]{1,0:T(2,128)(2,1)}, u32[]{:S(2)}) copy-start(bf16[1,128]{1,0:T(2,128)(2,1)} %constant.36.clone.1) | copy-start | bytes 772
  85.6 22.0 %copy-start.5 = (bf16[4,577,128]{2,1,0:T(8,128)(2,1)}, bf16[4,577,128]{2,1,0:T(8,128)(2,1)S(1)}, u32[]{:S(2)}) copy-start(bf16[4,577,128]{2,1,0:T(8,128)(2,1)S(1)} %all-gather.4) | copy-start | bytes 1772548
  105.0 1.8 copy-start.9
  132.8 4.0 %copy-start.15 = (bf16[4,1,128]{2,1,0:T(2,128)(2,1)S(1)}, bf16[4,1,128]{2,1,0:T(2,128)(2,1)}, u32[]{:S(2)}) copy-start(bf16[4,1,128]{2,1,0:T(2,128)(2,1)} %slice.279) | copy-start | bytes 3076
  152.8 3.0 %copy-start.8 = (bf16[1024,4,128]{0,2,1:T(8,128)(2,1)S(1)}, bf16[1024,4,128]{0,2,1:T(8,128)(2,1)}, u32[]{:S(2)}) copy-start(bf16[1024,4,128]{0,2,1:T(8,128)(2,1)} %reshape.486) | copy-start | bytes 3145732
  155.8 3.5 %copy-start.7 = (bf16[1024,512]{1,0:T(8,128)(2,1)S(1)}, bf16[1024,512]{1,0:T(8,128)(2,1)}, u32[]{:S(2)}) copy-start(bf16[1024,512]{1,0:T(8,128)(2,1)} %copy-done.6) | copy-start | bytes 3145732
  159.1 0.7 copy-start.13
  159.1 0.7 copy-start.14
  159.1 0.7 copy-start.22
  159.1 0.7 copy-start.23
  159.1 0.7 copy-start.24
  159.2 0.6 copy-start.25
  159.2 0.7 copy-start.26
  159.2 0.7 copy-start.27
  159.2 0.7 copy-start.28
  159.2 0.7 copy-start.29
  159.2 0.7 copy-start.30
  159.2 0.7 copy-start.31
  159.2 0.6 copy-start.32
  159.2 0.6 copy-start.33
  159.2 0.7 copy-start.34
  159.3 0.7 copy-start.35
  159.3 0.7 copy-start.36
  159.3 0.7 copy-start.37
  160.0 6.2 %copy-start.11 = (bf16[2,256,256]{2,1,0:T(8,128)(2,1)S(1)}, bf16[2,256,256]{2,1,0:T(8,128)(2,1)}, u32[]{:S(2)}) copy-start(bf16[2,256,256]{2,1,0:T(8,128)(2,1)} %param.23) | copy-start | bytes 786436
  166.1 0.7 copy-start.19
  167.0 2.4 %copy-start.4 = (f32[1024,512]{0,1:T(8,128)S(1)}, f32[1024,512]{0,1:T(8,128)}, u32[]{:S(2)}) copy-start(f32[1024,512]{0,1:T(8,128)} %copy.108) | copy-start | bytes 6291460
  167.0 2.4 %copy-start.21 = (f32[128]{0:T(128)S(1)}, f32[128]{0:T(128)}, u32[]{:S(2)}) copy-start(f32[128]{0:T(128)} %param.27) | copy-start | bytes 1540
  169.4 1.6 copy-start.10
  199.0 7.6 %copy-start.16 = (f32[1024]{0:T(1024)S(1)}, f32[1024]{0:T(1024)}, u32[]{:S(2)}) copy-start(f32[1024]{0:T(1024)} %param.31) | copy-start | bytes 12292
  199.0 7.6 %copy-start.17 = (f32[1024]{0:T(1024)S(1)}, f32[1024]{0:T(1024)}, u32[]{:S(2)}) copy-start(f32[1024]{0:T(1024)} %param.30) | copy-start | bytes 12292
